TPU v7x, 32 devices: a whole 2x2x4 slice. The times are simulated.
32 devices in a mesh: sp: 8 (over z, x), dp: 4 (over y, core).
Axes of the slice: x: 2, y: 2, z: 4, core: 2. Of those that a mesh axis runs over, the one named last changes fastest.
Arguments:
- query_input: bfloat16 [4, 4096, 2048], P('dp', 'sp'), may hold values from -6 to 6
- forget_gate_input: bfloat16 [4, 4096, 2048], P('dp', 'sp'), may hold values from -6.5 to 6.5
- value_input: bfloat16 [4, 4096, 2048], P('dp', 'sp'), may hold values from -6 to 6
- gate_input: bfloat16 [4, 4096, 2048], P('dp', 'sp'), may hold values from -6 to 6
- extra_decay: bfloat16 [4, 4096, 2048], P('dp', 'sp'), may hold values from -0.7 to 0
- floor_gap: float32 [2048], replicated, may hold values from 0 to 0.06
- norm_gain: float32 [2048], replicated, may hold values from 0.1 to 1.9
- out_weight: bfloat16 [2048, 4096], P(None, 'dp'), may hold values from -0.125 to 0.125
Outputs:
- mixed_out: bfloat16 [4, 4096, 4096], P('dp', 'sp')
All inputs are finite; a program needn't handle non-finite values.
Results may differ from a plain program's by a relative error of at most 0.0049.
Values may be sent and summed in bfloat16 or wider, within the bound.
A program may use at most 192 MiB of HBM per device.

v0:
```python
import jax
import jax.numpy as jnp
from jax import lax
from jax.sharding import PartitionSpec as P

HEAD_DIM = 128
BLOCK = 128


norm_eps = 1e-06
highest = lax.Precision.HIGHEST


def entering_2(value, axis, join, neutral):
    count, mine = (lax.axis_size(axis), lax.axis_index(axis))
    pieces = jax.tree.map(lambda part: lax.all_gather(part, axis), value)
    total = jax.tree.map(
        lambda part, zero: jnp.full_like(part, 0) + jnp.asarray(zero, part.dtype), value, neutral
    )

    def step(position, total):
        longer = join(total, jax.tree.map(lambda part: part[position], pieces))
        return jax.tree.map(lambda new, old: jnp.where(position < mine, new, old), longer, total)

    return lax.fori_loop(0, count - 1, step, total)


def prepare(query_input, forget_gate_input, value_input, extra_decay, floor_gap):
    positions, channels = query_input.shape
    head_shape = (positions, channels // HEAD_DIM, HEAD_DIM)
    queries = jax.nn.silu(query_input.astype(jnp.float32))
    inflow = floor_gap * jax.nn.sigmoid(-forget_gate_input.astype(jnp.float32))
    log_keep = jnp.log1p(-inflow) + extra_decay.astype(jnp.float32)
    value_rows = value_input.astype(jnp.float32)
    return (
        queries.reshape(head_shape),
        inflow.reshape(head_shape),
        log_keep.reshape(head_shape),
        value_rows.reshape(head_shape),
    )


def block_parts(queries, inflow, log_keep, value_rows):
    positions, head_count, head_width = queries.shape
    block_count = positions // BLOCK
    causal = jnp.tril(jnp.ones((BLOCK, BLOCK), dtype=bool))

    def to_pairs(tensor):
        paired = tensor.reshape(block_count, BLOCK, head_count, head_width).transpose(0, 2, 1, 3)
        return paired

    def group_terms(operands):
        query_grp, inflow_grp, keep_grp, value_grp = operands
        running = jnp.cumsum(keep_grp, axis=1)
        decayed = query_grp * jnp.exp(running)
        boosted = inflow_grp * jnp.exp(-running)
        scores = jnp.einsum("gtk,gsk->gts", decayed, boosted, precision=highest)
        scores = jnp.where(causal[None], scores, 0.0)
        inner = jnp.einsum("gts,gsv->gtv", scores, value_grp, precision=highest)
        latest = running[:, -1, :]
        weighted = inflow_grp * jnp.exp(latest[:, None, :] - running)
        block_state = jnp.einsum("gsk,gsv->gkv", weighted, value_grp, precision=highest)
        return (inner, decayed, block_state, jnp.exp(latest))

    inner, decayed, block_state, block_fade = lax.map(
        group_terms, (to_pairs(queries), to_pairs(inflow), to_pairs(log_keep), to_pairs(value_rows))
    )
    return (inner, decayed, block_state, block_fade)


def finish(inner, decayed, prior_states, gate_input, norm_gain):
    block_count, head_count, block_len, head_width = inner.shape
    result = inner + jnp.einsum("nhtk,nhkv->nhtv", decayed, prior_states, precision=highest)
    result = result.transpose(0, 2, 1, 3).reshape(block_count * block_len, head_count, head_width)
    scaled = result * lax.rsqrt(jnp.mean(result * result, axis=-1, keepdims=True) + norm_eps)
    scaled = scaled.reshape(block_count * block_len, head_count * head_width)
    scaled = scaled * norm_gain * jax.nn.silu(gate_input.astype(jnp.float32))
    return scaled.astype(jnp.bfloat16)


def link_states(earlier, follower):
    return (earlier[0] * follower[0], follower[0][..., None] * earlier[1] + follower[1])


def local_states(block_state, block_fade):
    fade_run, state_run = lax.associative_scan(link_states, (block_fade, block_state), axis=0)
    prior_local = jnp.concatenate([jnp.zeros_like(state_run[:1]), state_run[:-1]], axis=0)
    prior_fade = jnp.concatenate([jnp.ones_like(fade_run[:1]), fade_run[:-1]], axis=0)
    return (prior_local, prior_fade, fade_run[-1], state_run[-1])


def shards(
    query_input,
    forget_gate_input,
    value_input,
    gate_input,
    extra_decay,
    floor_gap,
    norm_gain,
    out_weight,
):
    queries, inflow, log_keep, value_rows = prepare(
        query_input[0], forget_gate_input[0], value_input[0], extra_decay[0], floor_gap
    )
    inner, decayed, block_state, block_fade = block_parts(queries, inflow, log_keep, value_rows)
    prior_local, prior_fade, whole_fade, whole_state = local_states(block_state, block_fade)
    entering = entering_2(
        (whole_fade, whole_state),
        "sp",
        link_states,
        (jnp.ones_like(whole_fade), jnp.zeros_like(whole_state)),
    )
    prior_states = prior_local + prior_fade[..., None] * entering[1][None]
    hidden = finish(inner, decayed, prior_states, gate_input[0], norm_gain)[None]
    mixed_out = jnp.einsum(
        "stw,wc->stc",
        hidden,
        lax.all_gather(out_weight, "dp", axis=1, tiled=True),
        preferred_element_type=jnp.float32,
    )
    return mixed_out.astype(jnp.bfloat16)


def solution(mesh):
    in_specs = (
        P("dp", "sp", None),
        P("dp", "sp", None),
        P("dp", "sp", None),
        P("dp", "sp", None),
        P("dp", "sp", None),
        P(),
        P(),
        P(None, "dp"),
    )
    out_specs = P("dp", "sp", None)
    return jax.shard_map(shards, mesh=mesh, in_specs=in_specs, out_specs=out_specs, check_vma=False)
```

profile of v0, /device:TPU:25, one launch (start us, length us, event | category | flops | bytes accessed | tf_op | source)
XLA Modules:
  0.0 369.0 jit_solution(5345971531514836039)
XLA Ops:
  20.9 3.0 fusion.21
  24.0 8.3 %fusion.27 = (f32[4,16,128,128]{3,1,2,0:T(8,128)}, f32[4,16,128,128]{3,1,2,0:T(8,128)}) fusion(f32[16,128]{1,0:T(8,128)S(1)} %bitcast.134, f32[4,128,16,128]{3,2,1,0:T(8,128)} %bitcast.131, f32[4,128,16,128]{3,2,1,0:T(8,128)} %bitcast.132), kind=kLoop, calls=%fused_computation.55 | loop fusion | flops 3145728 | bytes 16785408 | tf_op jit(solution)/shard_map/transpose | solution.py:49
  32.3 61.9 %while.31 = (s32[]{:T(128)}, f32[4,16,128,128]{2,3,1,0:T(8,128)}, f32[4,16,128,128]{3,2,1,0:T(8,128)}, f32[4,16,128,128]{3,2,1,0:T(8,128)}, f32[4,16,128]{2,1,0:...) while((s32[]{:T(128)}, f32[4,16,128,128]{2,3,1,0:T(8,128)}, ...), condition=%wide.region_2.3_spmd.clone, body=%wide.region_0.2_spmd.clone.sunk | while | flops 1243103232 | bytes 24193648 | solution.py:65
  40.1 3.0 fusion.58
  43.1 3.3 fusion.59
  55.7 3.0 fusion.58
  58.7 3.3 fusion.59
  71.1 3.0 fusion.58
  74.1 3.3 fusion.59
  86.6 3.0 fusion.58
  89.6 3.3 fusion.59
  98.4 11.8 %pad.75 = f32[3,16,128,128]{3,2,1,0:T(8,128)} pad(f32[2,16,128,128]{3,2,1,0:T(8,128)S(1)} %pad_add_fusion, f32[]{:T(128)} %constant.65.clone.1), padding=0_0_1x0_0_0x0_0_0x0_0_0 | pad | bytes 5242884
  113.3 12.2 %pad.31 = f32[4,16,128,128]{3,2,1,0:T(8,128)} pad(f32[2,16,128,128]{3,2,1,0:T(8,128)S(1)} %pad_add_fusion, f32[]{:T(128)} %constant.65.clone.1), padding=1_0_1x0_0_0x0_0_0x0_0_0 | pad | bytes 6291460 | tf_op jit(solution)/shard_map/pad | solution.py:86
  128.1 12.1 %pad.30 = f32[4,16,128,128]{3,2,1,0:T(8,128)} pad(f32[2,16,128,128]{3,2,1,0:T(8,128)S(1)} %pad_maximum_fusion, f32[]{:T(128)} %constant.65.clone.1), padding=0_1_1x0_0_0x0_0_0x0_0_0 | pad | bytes 6291460 | tf_op jit(solution)/shard_map/pad | solution.py:86
  140.2 22.5 %all_gather.9 = f32[8,16,128]{2,1,0:T(8,128)S(1)} all-gather(f32[1,16,128]{2,1,0:T(8,128)S(1)} %slice.134), channel_id=1, replica_groups=mesh['sp'=8,'dp'=4] {'sp'}, dimensions={0}, use_global_device_ids=true | all-gather | bytes 73728 | tf_op jit(solution)/shard_map/all_gather | solution.py:16
  162.7 5.2 %slice_add_fusion = f32[3,16,128,128]{3,2,1,0:T(8,128)} fusion(f32[4,16,128,128]{3,2,1,0:T(8,128)} %pad.31, f32[4,16,128,128]{3,2,1,0:T(8,128)} %pad.30), kind=kLoop, calls=%fused_computation.56 | loop fusion | flops 786432 | bytes 9437184 | tf_op jit(solution)/shard_map/add | solution.py:86
  167.9 68.9 %all-gather.3.cloned.1.call-done = f32[8,16,128,128]{3,2,1,0:T(8,128)} async-done(((f32[1,16,128,128]{3,2,1,0:T(8,128)}), f32[8,16,128,128]{3,2,1,0:T(8,128)}) %all-gather.3.cloned.1.call-update) | async-done | bytes 8388624 | tf_op jit(solution)/shard_map/all_gather | solution.py:16
  236.8 13.7 %while.32 = (s32[]{:T(128)}, f32[16,128,128]{2,1,0:T(8,128)S(1)}, s32[]{:T(128)}, f32[8,16,128]{2,1,0:T(8,128)S(1)}, f32[8,16,128,128]{3,2,1,0:T(8,128)}, /*index=5*/s32[]{:T(128)}, s32[]{:T(128)}) while((s32[]{:T(128)}, f32[16,128,128]{2,1,0:T(8,128)S(1)}, s32[]{:T(128)}, f32[8,16,128]{2,1,0:T(8,128)S(1)}, ...), condition=%wide.region_4.5_spmd.clone, body=%wide.region_3.4_spmd.clone.sunk | while | flops 1048580 | bytes 3170409 | solution.py:25
  250.5 16.6 %multiply_reduce_fusion = (f32[4,128,16]{1,2,0:T(8,128)S(1)}, f32[4,128,16,128]{1,3,2,0:T(8,128)}) fusion(f32[4,16,128,128]{2,3,1,0:T(8,128)} %get-tuple-element.154, f32[4,16,128,128]{3,2,1,0:T(8,128)} %get-tuple-element.155, f32[3,16,128,128]{3,2,1,0:T(8,128)} %slice_add_fusion, f32[16,128,128]{2,1,0:T(8,128)S(1)} %get-tuple-element.158, ...), kind=kOutput, calls=%fused_computation.47 | convolution fusion | flops 1615847424 | bytes 16842752 | tf_op jit(solution)/shard_map/nhtk,nhkv->nhtv/dot_general | solution.py:73
  269.9 4.9 %mul.168 = f32[1,512,2048]{2,1,0:T(8,128)} reshape(f32[512,16,128]{2,1,0:T(8,128)} %mul.167) | data formatting | bytes 8388608 | tf_op jit(solution)/shard_map/mul | solution.py:75
  274.8 5.5 %copy.38 = f32[4,128,16,128]{3,2,1,0:T(8,128)} copy(f32[4,128,16,128]{1,3,2,0:T(8,128)} %get-tuple-element.281) | data formatting | bytes 8388608 | tf_op jit(solution)/shard_map/transpose | solution.py:74
  280.3 5.1 %reshape.127 = f32[1,512,2048]{2,1,0:T(8,128)} reshape(f32[4,128,16,128]{3,2,1,0:T(8,128)} %copy.38) | data formatting | bytes 8388608 | tf_op jit(solution)/shard_map/reshape | solution.py:74
  285.4 59.3 %all-gather.5.cloned.1.call-done = bf16[2048,4096]{1,0:T(8,128)(2,1)} async-done(((bf16[2048,1024]{1,0:T(8,128)(2,1)}), bf16[2048,4096]{1,0:T(8,128)(2,1)}) %all-gather.5.cloned.1.call-update) | async-done | bytes 16777232 | tf_op jit(solution)/shard_map/all_gather | solution.py:118
  344.8 17.4 %fusion.12 = bf16[1,512,4096]{2,1,0:T(8,128)(2,1)} fusion(bf16[2048,4096]{1,0:T(8,128)(2,1)} %all-gather.5.cloned.1.call-done, bf16[1,512,2048]{2,1,0:T(8,128)(2,1)S(1)} %copy-done.5, f32[1,512,2048]{2,1,0:T(8,128)} %reshape.127, f32[1,512,2048]{2,1,0:T(8,128)} %mul.168, f32[2048]{0:T(1024)S(1)} %copy-done.6), kind=kOutput, calls=%fused_computation.27 | convolution fusion | flops 8601468928 | bytes 31465472 | tf_op jit(solution)/shard_map/stw,wc->stc/dot_general | solution.py:115
  (98 shorter events, 76.8 us)
Async XLA Ops:
  6.5 230.3 %all-gather.3.cloned.1.call-start = ((), (), s32[]{:S(2)}) async-start(), calls=%async_computation | async-start | bytes 9437184 | tf_op jit(solution)/shard_map/all_gather | solution.py:16
  9.2 2.9 copy-start.1
  12.6 2.9 copy-start.2
  17.0 2.4 copy-start.3
  20.9 3.1 copy-start.4
  97.2 1.0 copy-start
  112.6 232.2 %all-gather.5.cloned.1.call-start = ((), (), s32[]{:S(2)}) async-start(), calls=%async_computation.1 | async-start | bytes 20971520 | tf_op jit(solution)/shard_map/all_gather | solution.py:118
  280.3 64.4 %copy-start.5 = (bf16[1,512,2048]{2,1,0:T(8,128)(2,1)S(1)}, bf16[1,512,2048]{2,1,0:T(8,128)(2,1)}, u32[]{:S(2)}) copy-start(bf16[1,512,2048]{2,1,0:T(8,128)(2,1)} %param.15) | copy-start | bytes 6291460
  280.3 64.4 %copy-start.6 = (f32[2048]{0:T(1024)S(1)}, f32[2048]{0:T(1024)}, u32[]{:S(2)}) copy-start(f32[2048]{0:T(1024)} %param.18) | copy-start | bytes 24580
Sparse Core Ops, SparseCore 0:
  112.7 124.0 all-gather.2
  238.3 106.3 all-gather.4
where the time goes:
time: 371 us; the launch traced here: 369 us
  waiting for transfers between devices  129 us (35%)
  local copies, waits for them, and re-layouts  78.4 us (21%)
  matrix products  70.4 us (19%)
  other arithmetic  54.8 us (15%)
  blocking collectives  22.5 us (6%)
  between operations  13.6 us (4%)
    all_gather x1, waiting for transfers between devices, entering_2(): pieces = jax.tree.map(lambda part: lax.all_gather(part, axis), value)  68.9 us
    all_gather x1, waiting for transfers between devices, shards(): lax.all_gather(out_weight, 'dp', axis=1, tiled=True)  59.3 us
    pad x4, local copies, waits for them, and re-layouts, local_states(): lax.associative_scan(link_states, (block_fade, block_state), axis=0)  24.3 us
    all_gather x1, blocking collectives, entering_2(): pieces = jax.tree.map(lambda part: lax.all_gather(part, axis), value)  22.5 us
    unnamed x20, local copies, waits for them, and re-layouts  20.6 us
    dot_general x1, matrix products, shards(): jnp.einsum('stw,wc->stc', hidden, lax.all_gather(out_weight, 'dp', axis=1...  17.4 us
    dot_general x1, matrix products, finish(): jnp.einsum('nhtk,nhkv->nhtv', decayed, prior_states, precision=highest)  16.6 us
    select_n x7, other arithmetic, step(): jnp.where(position < mine, new, old)  13.5 us
  transfers between devices with their start and end apart: 2, of which 2 were waited for; matrix products, arithmetic and copies ran while one was open for 22% of the time, Pallas kernels for 0%

commit v1 on v0

v1 whole, which is shorter than its diff:
```python
import functools

import jax
import jax.numpy as jnp
from jax import lax
from jax.experimental import pallas as pl
from jax.experimental.pallas import tpu as pltpu
from jax.sharding import PartitionSpec as P

HEAD_DIM = 128
BLOCK = 128
GROUP = 2
norm_eps = 1e-06
bf16, f32 = jnp.bfloat16, jnp.float32


def dot(a, b, dims):
    return lax.dot_general(a, b, (dims, ((), ())), preferred_element_type=f32)


NN = ((1,), (0,))
NT = ((1,), (1,))
TN = ((0,), (0,))


def local_kernel(q_ref, f_ref, v_ref, e_ref, gap_ref, inner_ref, dec_ref, state_ref, fade_ref):
    positions, width = q_ref.shape
    rows = lax.broadcasted_iota(jnp.int32, (BLOCK, BLOCK), 0)
    cols = lax.broadcasted_iota(jnp.int32, (BLOCK, BLOCK), 1)
    causal = rows >= cols
    ones_tri = jnp.where(causal, 1.0, 0.0).astype(bf16)
    gap = gap_ref[...]
    states = [None] * (width // HEAD_DIM)
    total = jnp.zeros((1, width), f32)
    for block in range(positions // BLOCK):
        at = pl.ds(block * BLOCK, BLOCK)
        q_in = q_ref[at, :].astype(f32)
        queries = q_in / (1.0 + jnp.exp(-q_in))
        inflow = gap / (1.0 + jnp.exp(f_ref[at, :].astype(f32)))
        log_keep = jnp.log(1.0 - inflow) + e_ref[at, :].astype(f32)
        high = log_keep.astype(bf16)
        low = (log_keep - high.astype(f32)).astype(bf16)
        running = dot(ones_tri, high, NN) + dot(ones_tri, low, NN)
        latest = running[BLOCK - 1 :, :]
        decayed = queries * jnp.exp(running)
        boosted = (inflow * jnp.exp(-running)).astype(bf16)
        weighted = (inflow * jnp.exp(latest - running)).astype(bf16)
        dec_ref[at, :] = (decayed * jnp.exp(total)).astype(bf16)
        decayed = decayed.astype(bf16)
        fade = jnp.exp(latest)
        for head in range(width // HEAD_DIM):
            lanes = slice(head * HEAD_DIM, (head + 1) * HEAD_DIM)
            value = v_ref[at, lanes]
            scores = dot(decayed[:, lanes], boosted[:, lanes], NT)
            scores = jnp.where(causal, scores, 0.0).astype(bf16)
            inner = dot(scores, value, NN)
            fresh = dot(value, weighted[:, lanes], TN)
            if block:
                inner = inner + dot(decayed[:, lanes], states[head].astype(bf16), NT)
                fresh = fade[:, lanes] * states[head] + fresh
            states[head] = fresh
            inner_ref[at, lanes] = inner
        total = total + latest
    for head in range(width // HEAD_DIM):
        state_ref[head] = states[head].astype(bf16)
    fade_ref[...] = jnp.exp(total)


def finish_kernel(axis, inner_ref, dec_ref, gate_ref, gain_ref, states_ref, fades_ref, hidden_ref):
    positions, width = inner_ref.shape
    mine = lax.axis_index(axis)
    count = states_ref.shape[0]
    for head in range(width // HEAD_DIM):
        lanes = slice(head * HEAD_DIM, (head + 1) * HEAD_DIM)
        entering = jnp.zeros((HEAD_DIM, HEAD_DIM), f32)
        for other in range(count - 1):
            longer = fades_ref[other][:, lanes] * entering + states_ref[other, head].astype(f32)
            entering = jnp.where(other < mine, longer, entering)
        result = inner_ref[:, lanes] + dot(dec_ref[:, lanes], entering.astype(bf16), NT)
        mean = jnp.mean(result * result, axis=-1, keepdims=True)
        scaled = result * lax.rsqrt(mean + norm_eps) * gain_ref[:, lanes]
        gate = gate_ref[:, lanes].astype(f32)
        hidden_ref[:, lanes] = (scaled * (gate / (1.0 + jnp.exp(-gate)))).astype(bf16)


def project_kernel(hidden_ref, weight_ref, out_ref):
    pieces, _, depth, width = weight_ref.shape
    weight = weight_ref[...].reshape(pieces * depth, width)
    out_ref[...] = dot(hidden_ref[...], weight, NN).astype(out_ref.dtype)


def shards(
    query_input,
    forget_gate_input,
    value_input,
    gate_input,
    extra_decay,
    floor_gap,
    norm_gain,
    out_weight,
):
    sp, dp = lax.axis_size("sp"), lax.axis_size("dp")
    _, positions, channels = query_input.shape
    heads, width = channels // HEAD_DIM, GROUP * HEAD_DIM
    steps = heads // GROUP
    depth, columns = out_weight.shape
    piece = depth // sp

    mine = lax.dynamic_slice_in_dim(out_weight, lax.axis_index("sp") * piece, piece, axis=0)
    weights = lax.all_gather(mine, ("sp", "dp")).reshape(sp, dp, piece, columns)

    tokens = pl.BlockSpec((positions, width), lambda i: (0, i))
    params = pl.BlockSpec((1, width), lambda i: (0, i))
    state = pl.BlockSpec((GROUP, HEAD_DIM, HEAD_DIM), lambda i: (i, 0, 0))
    inner, decayed, whole_state, whole_fade = pl.pallas_call(
        local_kernel,
        grid=(steps,),
        in_specs=[tokens] * 4 + [params],
        out_specs=[tokens, tokens, state, params],
        out_shape=[
            jax.ShapeDtypeStruct((positions, channels), f32),
            jax.ShapeDtypeStruct((positions, channels), bf16),
            jax.ShapeDtypeStruct((heads, HEAD_DIM, HEAD_DIM), bf16),
            jax.ShapeDtypeStruct((1, channels), f32),
        ],
        cost_estimate=pl.CostEstimate(flops=3 * 10**9, bytes_accessed=2 * 10**7, transcendentals=10**7),
        name="local",
    )(query_input[0], forget_gate_input[0], value_input[0], extra_decay[0], floor_gap[None])

    states = lax.all_gather(whole_state, "sp")
    fades = lax.all_gather(whole_fade, "sp")

    hidden = pl.pallas_call(
        functools.partial(finish_kernel, "sp"),
        grid=(steps,),
        in_specs=[
            tokens,
            tokens,
            tokens,
            params,
            pl.BlockSpec((sp, GROUP, HEAD_DIM, HEAD_DIM), lambda i: (0, i, 0, 0)),
            pl.BlockSpec((sp, 1, width), lambda i: (0, 0, i)),
        ],
        out_specs=tokens,
        out_shape=jax.ShapeDtypeStruct((positions, channels), bf16),
        cost_estimate=pl.CostEstimate(flops=10**9, bytes_accessed=10**7, transcendentals=10**6),
        name="finish",
    )(inner, decayed, gate_input[0], norm_gain[None], states, fades)

    tile = columns // 2
    mixed = pl.pallas_call(
        project_kernel,
        grid=(dp, columns // tile),
        in_specs=[
            pl.BlockSpec((positions, channels), lambda n, c: (0, 0)),
            pl.BlockSpec((sp, 1, piece, tile), lambda n, c: (0, n, 0, c)),
        ],
        out_specs=pl.BlockSpec((positions, tile), lambda n, c: (0, n * (columns // tile) + c)),
        out_shape=jax.ShapeDtypeStruct((positions, dp * columns), bf16),
        name="project",
    )(hidden, weights)
    return mixed[None]


def solution(mesh):
    in_specs = (
        P("dp", "sp", None),
        P("dp", "sp", None),
        P("dp", "sp", None),
        P("dp", "sp", None),
        P("dp", "sp", None),
        P(),
        P(),
        P(None, "dp"),
    )
    out_specs = P("dp", "sp", None)
    return jax.shard_map(shards, mesh=mesh, in_specs=in_specs, out_specs=out_specs, check_vma=False)
```

time: 371 us -> 236 us (0.64)
  local copies, waits for them, and re-layouts: 78.4 us -> 1.92 us
  matrix products: 70.4 us -> 0 us
  other arithmetic: 54.8 us -> 0 us
  Pallas kernels: 0 us -> 39.8 us
  waiting for transfers between devices: 129 us -> 153 us
    dot_general x14 -> x0, matrix products: 70.4 us -> none  [the longest x1 17.4 us: shards(): jnp.einsum('stw,wc->stc', hidden, lax.all_gather(out_weight, 'dp', axis=1...]
    pallas_call x0 -> x3, Pallas kernels: none -> 39.8 us  [the longest x1 15.1 us: shards(): pl.pallas_call(project_kernel, grid=(dp, columns // tile), in_specs=[pl.B...]
    pad x4 -> x0, local copies, waits for them, and re-layouts: 24.3 us -> none  [local_states(): lax.associative_scan(link_states, (block_fade, block_state), axis=0)]
    all_gather x2, waiting for transfers between devices: 128 us -> 153 us  [the longest x1 106 us: shards(): weights = lax.all_gather(mine, ('sp', 'dp')).reshape(sp, dp, piece, columns)]
    unnamed x20 -> x2, local copies, waits for them, and re-layouts: 20.6 us -> 0.01 us
    select_n x7 -> x0, other arithmetic: 13.5 us -> none  [step(): jnp.where(position < mine, new, old)]
    transpose x2 -> x0, other arithmetic: 11.4 us -> none  [to_pairs(): tensor.reshape(block_count, BLOCK, head_count, head_width)]
    add x6 -> x0, other arithmetic: 8.33 us -> none  [the longest x4 5.39 us: local_states(): lax.associative_scan(link_states, (block_fade, block_state), axis=0)]
  transfers between devices with their start and end apart: 2 -> 2, of which waited for: 2 -> 2; matrix products, arithmetic and copies ran while one was open for 22% -> 1% of each run, Pallas kernels for 0% -> 4%
where the time goes in v1:
time: 236 us; the launch traced here: 232 us
  waiting for transfers between devices  153 us (65%)
  Pallas kernels  39.8 us (17%)
  blocking collectives  24.3 us (10%)
  between operations  13.4 us (6%)
    all_gather x1, waiting for transfers between devices, shards(): weights = lax.all_gather(mine, ('sp', 'dp')).reshape(sp, dp, piece, columns)  106 us
    all_gather x1, waiting for transfers between devices, shards(): states = lax.all_gather(whole_state, 'sp')  46.4 us
    all_gather x1, blocking collectives, shards(): fades = lax.all_gather(whole_fade, 'sp')  24.3 us
    pallas_call x1, Pallas kernels, shards(): pl.pallas_call(project_kernel, grid=(dp, columns // tile), in_specs=[pl.B...  15.1 us
    pallas_call x1, Pallas kernels, shards(): pl.pallas_call(local_kernel, grid=(steps,), in_specs=[tokens] * 4 + [para...  14.8 us
    pallas_call x1, Pallas kernels, shards(): pl.pallas_call(functools.partial(finish_kernel, 'sp'), grid=(steps,), in_...  9.87 us
  transfers between devices with their start and end apart: 2, of which 2 were waited for; matrix products, arithmetic and copies ran while one was open for 1% of the time, Pallas kernels for 4%

profile of v1, /device:TPU:25, one launch (start us, length us, event | category | flops | bytes accessed | tf_op | source)
XLA Modules:
  0.0 232.1 jit_solution(14410906787025077414)
XLA Ops:
  6.5 0.0 all-gather.7.cloned.1.call-start
  6.5 14.8 %local.1 = (f32[512,2048]{1,0:T(8,128)}, bf16[512,2048]{1,0:T(8,128)(2,1)}, bf16[16,128,128]{2,1,0:T(8,128)(2,1)}, f32[1,2048]{1,0:T(1,128)}) custom-call(bf16[512,2048]{1,0:T(8,128)(2,1)} %bitcast.16, bf16[512,2048]{1,0:T(8,128)(2,1)} %bitcast.17, bf16[512,2048]{1,0:T(8,128)(2,1)} %bitcast.18, bf16[512,2048]{1,0:T(8,128)(2,1)} %bitcast.19, f32[1,2048]{1,0:T(1,128)} %bitcast.20), custom_call_target="tpu_custom_call" | custom-call | flops 3000000000 | bytes 20000000 | tf_op jit(solution)/shard_map/local/pallas_call | solution.py:115
  21.4 0.0 copy-start
  21.4 0.0 all-gather.7.cloned.1.call-update
  21.4 0.0 all-gather.9.cloned.1.call-start
  21.5 1.9 constant_dynamic-slice_fusion
  23.4 0.0 all-gather.9.cloned.1.call-update
  23.4 0.0 copy-done
  23.4 24.3 %all-gather.3.fades_ref = f32[8,1,2048]{2,1,0:T(1,128)} all-gather(f32[1,1,2048]{2,1,0:T(1,128)S(1)} %bitcast.15), channel_id=3, replica_groups=mesh['sp'=8,'dp'=4] {'sp'}, dimensions={0}, use_global_device_ids=true | all-gather | bytes 73728 | tf_op jit(solution)/shard_map/all_gather | solution.py:131
  47.7 46.4 %all-gather.7.cloned.1.call-done = bf16[128,128,128]{2,1,0:T(8,128)(2,1)} async-done(((bf16[16,128,128]{2,1,0:T(8,128)(2,1)}), bf16[128,128,128]{2,1,0:T(8,128)(2,1)}) %all-gather.7.cloned.1.call-update) | async-done | bytes 4194320 | tf_op jit(solution)/shard_map/all_gather | solution.py:130
  94.1 9.9 %finish.1.hidden_ref = bf16[512,2048]{1,0:T(8,128)(2,1)} custom-call(f32[512,2048]{1,0:T(8,128)} %get-tuple-element.9.inner_ref, bf16[512,2048]{1,0:T(8,128)(2,1)} %get-tuple-element.10.dec_ref, bf16[512,2048]{1,0:T(8,128)(2,1)} %bitcast.13, f32[1,2048]{1,0:T(1,128)} %bitcast.14, bf16[8,16,128,128]{3,2,1,0:T(8,128)(2,1)} %bitcast.12, ...), custom_call_target="tpu_custom_call" | custom-call | flops 1000000000 | bytes 10000000 | tf_op jit(solution)/shard_map/finish/pallas_call | solution.py:133
  104.0 106.1 %all-gather.9.cloned.1.call-done = bf16[8192,1024]{1,0:T(8,128)(2,1)} async-done(((bf16[256,1024]{1,0:T(8,128)(2,1)}), bf16[8192,1024]{1,0:T(8,128)(2,1)}) %all-gather.9.cloned.1.call-update) | async-done | bytes 16777232 | tf_op jit(solution)/shard_map/all_gather | solution.py:110
  210.1 15.1 %project.1 = bf16[512,4096]{1,0:T(8,128)(2,1)} custom-call(bf16[512,2048]{1,0:T(8,128)(2,1)} %finish.1.hidden_ref, bf16[8,4,256,1024]{3,2,1,0:T(8,128)(2,1)} %bitcast.11), custom_call_target="tpu_custom_call" | custom-call | tf_op jit(solution)/shard_map/project/pallas_call | solution.py:151
Async XLA Ops:
  6.5 87.6 %all-gather.7.cloned.1.call-start = ((), (), s32[]{:S(2)}) async-start(), calls=%async_computation | async-start | bytes 4718592 | tf_op jit(solution)/shard_map/all_gather | solution.py:130
  21.4 2.0 copy-start
  21.4 188.7 %all-gather.9.cloned.1.call-start = ((), (), s32[]{:S(2)}) async-start(), calls=%async_computation.1 | async-start | bytes 17301504 | tf_op jit(solution)/shard_map/all_gather | solution.py:110
Sparse Core Ops, SparseCore 0:
  21.5 72.5 all-gather.6
  97.0 113.0 all-gather.8

commit v2 on v1

v2 whole, which is shorter than its diff:
```python
import functools

import jax
import jax.numpy as jnp
from jax import lax
from jax.experimental import pallas as pl
from jax.experimental.pallas import tpu as pltpu
from jax.sharding import PartitionSpec as P

HEAD_DIM = 128
BLOCK = 128
GROUP = 2
CORES = 2
CHUNKS = 8
FADE_ROWS = 16
norm_eps = 1e-06
bf16, f32 = jnp.bfloat16, jnp.float32


def dot(a, b, dims):
    return lax.dot_general(a, b, (dims, ((), ())), preferred_element_type=f32)


NN = ((1,), (0,))
NT = ((1,), (1,))
TN = ((0,), (0,))


def local_part(q_ref, f_ref, v_ref, e_ref, gap_ref, inner_ref, dec_ref, states_ref, step):
    positions, width = q_ref.shape
    rows = lax.broadcasted_iota(jnp.int32, (BLOCK, BLOCK), 0)
    cols = lax.broadcasted_iota(jnp.int32, (BLOCK, BLOCK), 1)
    causal = rows >= cols
    ones_tri = jnp.where(causal, 1.0, 0.0).astype(bf16)
    gap = gap_ref[...]
    states = [None] * GROUP
    total = jnp.zeros((1, width), f32)
    for block in range(positions // BLOCK):
        at = pl.ds(block * BLOCK, BLOCK)
        q_in = q_ref[at, :].astype(f32)
        queries = q_in / (1.0 + jnp.exp(-q_in))
        inflow = gap / (1.0 + jnp.exp(f_ref[at, :].astype(f32)))
        log_keep = jnp.log(1.0 - inflow) + e_ref[at, :].astype(f32)
        high = log_keep.astype(bf16)
        low = (log_keep - high.astype(f32)).astype(bf16)
        running = dot(ones_tri, high, NN) + dot(ones_tri, low, NN)
        latest = running[BLOCK - 1 :, :]
        decayed = queries * jnp.exp(running)
        boosted = (inflow * jnp.exp(-running)).astype(bf16)
        weighted = (inflow * jnp.exp(latest - running)).astype(bf16)
        dec_ref[step, at, :] = (decayed * jnp.exp(total)).astype(bf16)
        decayed = decayed.astype(bf16)
        fade = jnp.exp(latest)
        for head in range(GROUP):
            lanes = slice(head * HEAD_DIM, (head + 1) * HEAD_DIM)
            value = v_ref[at, lanes]
            scores = dot(decayed[:, lanes], boosted[:, lanes], NT)
            scores = jnp.where(causal, scores, 0.0).astype(bf16)
            inner = dot(scores, value, NN)
            fresh = dot(value, weighted[:, lanes], TN)
            if block:
                inner = inner + dot(decayed[:, lanes], states[head].astype(bf16), NT)
                fresh = fade[:, lanes] * states[head] + fresh
            states[head] = fresh
            inner_ref[step, at, lanes] = inner
        total = total + latest
    fade = jnp.exp(total)
    high = fade.astype(bf16).astype(f32)
    first = lax.broadcasted_iota(jnp.int32, (FADE_ROWS, width), 0) == 0
    fade = jnp.where(first, high, fade - high).astype(bf16)
    for head in range(GROUP):
        lanes = slice(head * HEAD_DIM, (head + 1) * HEAD_DIM)
        states_ref[step * GROUP + head, :HEAD_DIM, :] = states[head].astype(bf16)
        states_ref[step * GROUP + head, HEAD_DIM:, :] = fade[:, lanes]


def finish_part(gate_ref, gain_ref, inner_ref, dec_ref, enter_ref, hidden_ref, step):
    sp, own_heads = enter_ref.shape[:2]
    mine = lax.axis_index("sp")
    for head in range(GROUP):
        lanes = slice(head * HEAD_DIM, (head + 1) * HEAD_DIM)
        number = step * GROUP + head
        slot = lax.rem(mine - number // own_heads + sp, sp)
        entering = enter_ref[slot, lax.rem(number, own_heads)]
        result = inner_ref[step, :, lanes] + dot(dec_ref[step, :, lanes], entering, NT)
        mean = jnp.mean(result * result, axis=-1, keepdims=True)
        scaled = result * lax.rsqrt(mean + norm_eps) * gain_ref[:, lanes]
        gate = gate_ref[:, lanes].astype(f32)
        hidden_ref[:, lanes] = (scaled * (gate / (1.0 + jnp.exp(-gate)))).astype(bf16)


def remote(src, dst, send, recv, device):
    return pltpu.make_async_remote_copy(
        src_ref=src,
        dst_ref=dst,
        send_sem=send,
        recv_sem=recv,
        device_id=device,
        device_id_type=pl.DeviceIdType.MESH,
    )


def fused_kernel(
    sp,
    dp,
    q_ref,
    f_ref,
    v_ref,
    e_ref,
    gate_ref,
    gap_ref,
    gain_ref,
    w_ref,
    hidden_ref,
    all_ref,
    inner_ref,
    dec_ref,
    states_ref,
    given_ref,
    prior_ref,
    enter_ref,
    local_sem,
    own_sems,
    y_send,
    y_recv,
    x_send,
    x_recv,
    s1_send,
    s1_recv,
    s2_send,
    s2_recv,
    a_send,
    a_recv,
    b_send,
    b_recv,
):
    now = pl.program_id(0)
    last = pl.num_programs(0) - 1
    steps = inner_ref.shape[0]
    own_heads = given_ref.shape[1]
    i, j = lax.axis_index("sp"), lax.axis_index("dp")
    far = dp // CORES
    y, core = j // CORES, lax.rem(j, CORES)
    half = lax.rem(i, 2)
    partner = i + 1 - 2 * half
    sibling = y * CORES + 1 - core
    depth = w_ref.shape[0]
    chunk = depth // 2 // CHUNKS

    def rows(side, k):
        return pl.ds(pl.multiple_of(side * (depth // 2) + k * chunk, chunk), chunk)

    def block_of(offset, of_core):
        return lax.rem(y - offset + far, far) * CORES + of_core

    def over_y(offset, k):
        to = lax.rem(y + offset, far) * CORES + core
        at = rows(half, k)
        sems = (y_send.at[offset - 1, k], y_recv.at[offset - 1, k])
        return remote(w_ref.at[at], all_ref.at[j, at], *sems, {"sp": i, "dp": to})

    def forward(offset, k, side, of_core, send, recv, device):
        piece = all_ref.at[block_of(offset, of_core), rows(side, k)]
        return remote(piece, piece, send.at[offset - 1, k], recv.at[offset - 1, k], device)

    over_x = lambda o, k, side: forward(o, k, side, core, x_send, x_recv, {"sp": partner, "dp": j})
    beside = {"sp": i, "dp": sibling}
    near = lambda o, k, of_core: forward(o, k, half, of_core, s1_send, s1_recv, beside)
    other = lambda o, k, of_core: forward(o, k, 1 - half, of_core, s2_send, s2_recv, beside)
    own_near = remote(w_ref, all_ref.at[j], own_sems.at[0], own_sems.at[1], beside)
    from_near = remote(w_ref, all_ref.at[sibling], own_sems.at[0], own_sems.at[1], beside)
    keep = pltpu.make_async_copy(w_ref, all_ref.at[j], local_sem)
    pieces = [(o, k) for k in range(CHUNKS) for o in range(1, far)]

    def give(d):
        to = lax.rem(i + d, sp)
        part = states_ref.at[pl.ds(to * own_heads, own_heads)]
        return remote(part, given_ref.at[d], a_send.at[d], a_recv.at[d], {"sp": to, "dp": j})

    def back(d):
        to = lax.rem(i + d, sp)
        return remote(prior_ref.at[d], enter_ref.at[d], b_send.at[d], b_recv.at[d], {"sp": to, "dp": j})

    @pl.when(now == 0)
    def _():
        barrier = pltpu.get_barrier_semaphore()
        for o in range(1, far):
            to = lax.rem(y + o, far) * CORES + core
            pl.semaphore_signal(barrier, 1, device_id={"sp": i, "dp": to}, device_id_type=pl.DeviceIdType.MESH)
        pl.semaphore_signal(barrier, 1, device_id=beside, device_id_type=pl.DeviceIdType.MESH)
        for d in range(1, sp):
            to = lax.rem(i + d, sp)
            pl.semaphore_signal(barrier, 1, device_id={"sp": to, "dp": j}, device_id_type=pl.DeviceIdType.MESH)
        pl.semaphore_wait(barrier, far - 1 + 1 + sp - 1)
        for o, k in pieces:
            over_y(o, k).start()
        own_near.start()
        keep.start()

    @pl.when(now < steps)
    def _():
        local_part(q_ref, f_ref, v_ref, e_ref, gap_ref, inner_ref, dec_ref, states_ref, now)

    @pl.when(now == steps)
    def _():
        for d in range(1, sp):
            give(d).start()
        given_ref[0] = states_ref[pl.ds(i * own_heads, own_heads)]
        for d in range(1, sp):
            give(d).wait_recv()
        for head in range(own_heads):
            entering = jnp.zeros((HEAD_DIM, HEAD_DIM), f32)
            for source in range(sp):
                prior_ref[lax.rem(source - i + sp, sp), head] = entering.astype(bf16)
                slot = lax.rem(i - source + sp, sp)
                fade = given_ref[slot, head, HEAD_DIM:, :].astype(f32)
                fade = fade[0:1] + fade[1:2]
                entering = fade * entering + given_ref[slot, head, :HEAD_DIM, :].astype(f32)
        for d in range(1, sp):
            back(d).start()
        enter_ref[0] = prior_ref[0]
        for d in range(1, sp):
            back(d).wait_recv()

    @pl.when(now >= steps)
    def _():
        finish_part(gate_ref, gain_ref, inner_ref, dec_ref, enter_ref, hidden_ref, now - steps)

    for k in range(CHUNKS):
        @pl.when(now == min(2 * steps - 1, 2 * steps * k // CHUNKS + 3))
        def _():
            for o in range(1, far):
                over_y_in = forward(o, k, half, core, y_send, y_recv, beside)
                over_y_in.wait_recv()
                over_x(o, k, half).start()
                near(o, k, core).start()

    @pl.when(now == last)
    def _():
        for o, k in pieces:
            over_x(o, k, 1 - half).wait_recv()
            other(o, k, core).start()
        keep.wait()
        own_near.wait_send()
        from_near.wait_recv()
        for o, k in pieces:
            over_y(o, k).wait_send()
            over_x(o, k, half).wait_send()
            near(o, k, core).wait_send()
            near(o, k, 1 - core).wait_recv()
        for d in range(1, sp):
            give(d).wait_send()
            back(d).wait_send()
        for o, k in pieces:
            other(o, k, core).wait_send()
            other(o, k, 1 - core).wait_recv()


def project_kernel(hidden_ref, weight_ref, out_ref):
    out_ref[...] = dot(hidden_ref[...], weight_ref[0], NN).astype(out_ref.dtype)


def shards(
    query_input,
    forget_gate_input,
    value_input,
    gate_input,
    extra_decay,
    floor_gap,
    norm_gain,
    out_weight,
):
    sp, dp = lax.axis_size("sp"), lax.axis_size("dp")
    _, positions, channels = query_input.shape
    heads, width = channels // HEAD_DIM, GROUP * HEAD_DIM
    steps, own_heads = heads // GROUP, heads // sp
    depth, columns = out_weight.shape
    far = dp // CORES

    early = lambda s: (0, jnp.minimum(s, steps - 1))
    late = lambda s: (0, jnp.maximum(s - steps, 0))
    tokens = pl.BlockSpec((positions, width), early)
    after = pl.BlockSpec((positions, width), late)
    dma = pltpu.SemaphoreType.DMA
    flow = [dma((max(far - 1, 1), CHUNKS))] * 8
    packed = HEAD_DIM + FADE_ROWS
    hidden, weights = pl.pallas_call(
        functools.partial(fused_kernel, sp, dp),
        grid=(2 * steps,),
        in_specs=[tokens] * 4
        + [
            after,
            pl.BlockSpec((1, width), early),
            pl.BlockSpec((1, width), late),
            pl.BlockSpec((depth, columns), lambda s: (0, 0)),
        ],
        out_specs=[after, pl.BlockSpec(memory_space=pl.ANY)],
        out_shape=[
            jax.ShapeDtypeStruct((positions, channels), bf16),
            jax.ShapeDtypeStruct((dp, depth, columns), bf16),
        ],
        scratch_shapes=[
            pltpu.VMEM((steps, positions, width), f32),
            pltpu.VMEM((steps, positions, width), bf16),
            pltpu.VMEM((heads, packed, HEAD_DIM), bf16),
            pltpu.VMEM((sp, own_heads, packed, HEAD_DIM), bf16),
            pltpu.VMEM((sp, own_heads, HEAD_DIM, HEAD_DIM), bf16),
            pltpu.VMEM((sp, own_heads, HEAD_DIM, HEAD_DIM), bf16),
            dma,
            dma((2,)),
            *flow,
            *[dma((sp,))] * 4,
        ],
        compiler_params=pltpu.CompilerParams(
            collective_id=0,
            has_side_effects=True,
            dimension_semantics=("arbitrary",),
            vmem_limit_bytes=48 * 2**20,
        ),
        name="fused",
    )(
        query_input[0],
        forget_gate_input[0],
        value_input[0],
        extra_decay[0],
        gate_input[0],
        floor_gap[None],
        norm_gain[None],
        out_weight,
    )

    parts = 2
    tile = columns // parts
    mixed = pl.pallas_call(
        project_kernel,
        grid=(dp, parts),
        in_specs=[
            pl.BlockSpec((positions, channels), lambda n, c: (0, 0)),
            pl.BlockSpec((1, depth, tile), lambda n, c: (n, 0, c)),
        ],
        out_specs=pl.BlockSpec((positions, tile), lambda n, c: (0, n * parts + c)),
        out_shape=jax.ShapeDtypeStruct((positions, dp * columns), bf16),
        name="project",
    )(hidden, weights)
    return mixed[None]


def solution(mesh):
    in_specs = (
        P("dp", "sp", None),
        P("dp", "sp", None),
        P("dp", "sp", None),
        P("dp", "sp", None),
        P("dp", "sp", None),
        P(),
        P(),
        P(None, "dp"),
    )
    out_specs = P("dp", "sp", None)
    return jax.shard_map(shards, mesh=mesh, in_specs=in_specs, out_specs=out_specs, check_vma=False)
```

time: 236 us -> 107 us (0.45); the launches traced: 232 us -> 106 us
  waiting for transfers between devices: 153 us -> 0 us
  Pallas kernels: 39.8 us -> 102 us
  blocking collectives: 24.3 us -> 0 us
  between operations: 13.4 us -> 0.02 us
  local copies, waits for them, and re-layouts: 1.92 us -> 4.3 us
    all_gather x2 -> x0, waiting for transfers between devices: 153 us -> none  [the longest x1 106 us: shards(): weights = lax.all_gather(mine, ('sp', 'dp')).reshape(sp, dp, piece, columns)]
    pallas_call x3 -> x2, Pallas kernels: 39.8 us -> 102 us  [the longest x1 86.7 us: shards(): pl.pallas_call(functools.partial(fused_kernel, sp, dp), grid=(2 * steps,)...]
    all_gather x1 -> x0, blocking collectives: 24.3 us -> none  [shards(): fades = lax.all_gather(whole_fade, 'sp')]
    unnamed x2 -> x8, local copies, waits for them, and re-layouts: 0.01 us -> 4.3 us
  transfers between devices with their start and end apart: 2 -> 0, of which waited for: 2 -> 0; matrix products, arithmetic and copies ran while one was open for 1% -> 0% of each run, Pallas kernels for 4% -> 0%
where the time goes in v2:
time: 107 us; the launch traced here: 106 us
  Pallas kernels  102 us (95%)
  local copies, waits for them, and re-layouts  4.3 us (4%)
    pallas_call x1, Pallas kernels, shards(): pl.pallas_call(functools.partial(fused_kernel, sp, dp), grid=(2 * steps,)...  86.7 us
    pallas_call x1, Pallas kernels, shards(): pl.pallas_call(project_kernel, grid=(dp, parts), in_specs=[pl.BlockSpec((...  15 us
    unnamed x8, local copies, waits for them, and re-layouts  4.3 us

profile of v2, /device:TPU:25, one launch (start us, length us, event | category | flops | bytes accessed | tf_op | source)
XLA Modules:
  0.0 106.1 jit_solution(10156244441834798296)
XLA Ops:
  0.0 0.0 copy-start
  0.0 1.6 %copy-done = bf16[1,512,2048]{2,1,0:T(8,128)(2,1)S(1)} copy-done((bf16[1,512,2048]{2,1,0:T(8,128)(2,1)S(1)}, bf16[1,512,2048]{2,1,0:T(8,128)(2,1)}, u32[]{:S(2)}) %copy-start) | copy-done | bytes 2097176
  1.6 0.0 copy-start.2
  1.6 0.7 copy-done.2
  2.3 0.0 copy-start.3
  2.3 0.7 copy-done.3
  3.0 86.7 %fused.1 = (bf16[512,2048]{1,0:T(8,128)(2,1)S(1)}, bf16[4,2048,1024]{2,1,0:T(8,128)(2,1)}) custom-call(bf16[512,2048]{1,0:T(8,128)(2,1)S(1)} %bitcast.8, bf16[512,2048]{1,0:T(8,128)(2,1)} %bitcast.11, bf16[512,2048]{1,0:T(8,128)(2,1)} %bitcast.12, bf16[512,2048]{1,0:T(8,128)(2,1)} %bitcast.13, bf16[512,2048]{1,0:T(8,128)(2,1)} %bitcast.14, ...), custom_call_target="tpu_custom_call" | custom-call | tf_op jit(solution)/shard_map/fused/pallas_call | solution.py:287
  89.7 0.0 copy-start.1
  89.7 1.3 %copy-done.1 = bf16[512,2048]{1,0:T(8,128)(2,1)} copy-done((bf16[512,2048]{1,0:T(8,128)(2,1)}, bf16[512,2048]{1,0:T(8,128)(2,1)S(1)}, u32[]{:S(2)}) %copy-start.1) | copy-done | bytes 2097176
  91.1 15.0 %project.1 = bf16[512,4096]{1,0:T(8,128)(2,1)} custom-call(bf16[512,2048]{1,0:T(8,128)(2,1)} %copy-done.1, bf16[4,2048,1024]{2,1,0:T(8,128)(2,1)} %get-tuple-element.8.weight_ref), custom_call_target="tpu_custom_call" | custom-call | tf_op jit(solution)/shard_map/project/pallas_call | solution.py:334
Async XLA Ops:
  0.0 1.6 %copy-start = (bf16[1,512,2048]{2,1,0:T(8,128)(2,1)S(1)}, bf16[1,512,2048]{2,1,0:T(8,128)(2,1)}, u32[]{:S(2)}) copy-start(bf16[1,512,2048]{2,1,0:T(8,128)(2,1)} %param.8) | copy-start | bytes 6291460
  1.6 0.7 copy-start.2
  2.3 0.7 copy-start.3
  89.7 1.3 %copy-start.1 = (bf16[512,2048]{1,0:T(8,128)(2,1)}, bf16[512,2048]{1,0:T(8,128)(2,1)S(1)}, u32[]{:S(2)}) copy-start(bf16[512,2048]{1,0:T(8,128)(2,1)S(1)} %get-tuple-element.7.hidden_ref) | copy-start | bytes 6291460

commit v3 on v2

--- a/solution.py
+++ b/solution.py
@@ -315,7 +315,7 @@
             collective_id=0,
             has_side_effects=True,
             dimension_semantics=("arbitrary",),
-            vmem_limit_bytes=48 * 2**20,
+            vmem_limit_bytes=63 * 2**20,
         ),
         name="fused",
     )(
@@ -340,6 +340,7 @@
         ],
         out_specs=pl.BlockSpec((positions, tile), lambda n, c: (0, n * parts + c)),
         out_shape=jax.ShapeDtypeStruct((positions, dp * columns), bf16),
+        compiler_params=pltpu.CompilerParams(vmem_limit_bytes=63 * 2**20),
         name="project",
     )(hidden, weights)
     return mixed[None]

time: 107 us -> 103 us (0.963)
  local copies, waits for them, and re-layouts: 4.3 us -> 0 us
    unnamed x8 -> x0, local copies, waits for them, and re-layouts: 4.3 us -> none
where the time goes in v3:
time: 103 us
  Pallas kernels  103 us (100%)
    pallas_call x1, Pallas kernels, shards(): pl.pallas_call(functools.partial(fused_kernel, sp, dp), grid=(2 * steps,)...  87.8 us
    pallas_call x1, Pallas kernels, shards(): pl.pallas_call(project_kernel, grid=(dp, parts), in_specs=[pl.BlockSpec((...  15 us

profile of v3, /device:TPU:25, one launch (start us, length us, event | category | flops | bytes accessed | tf_op | source)
XLA Modules:
  0.0 102.8 jit_solution(7802305290163469240)
XLA Ops:
  0.0 87.8 %fused.1 = (bf16[512,2048]{1,0:T(8,128)(2,1)}, bf16[4,2048,1024]{2,1,0:T(8,128)(2,1)}) custom-call(bf16[512,2048]{1,0:T(8,128)(2,1)} %bitcast.8, bf16[512,2048]{1,0:T(8,128)(2,1)} %bitcast.9, bf16[512,2048]{1,0:T(8,128)(2,1)} %bitcast.10, bf16[512,2048]{1,0:T(8,128)(2,1)} %bitcast.11, bf16[512,2048]{1,0:T(8,128)(2,1)} %bitcast.12, f32[1,2048]{1,0:T(1,128)} %bitcast.13, ...), custom_call_target="tpu_custom_call" | custom-call | tf_op jit(solution)/shard_map/fused/pallas_call | solution.py:287
  87.8 15.0 %project.1 = bf16[512,4096]{1,0:T(8,128)(2,1)} custom-call(bf16[512,2048]{1,0:T(8,128)(2,1)} %get-tuple-element.7.hidden_ref, bf16[4,2048,1024]{2,1,0:T(8,128)(2,1)} %get-tuple-element.8.weight_ref), custom_call_target="tpu_custom_call" | custom-call | tf_op jit(solution)/shard_map/project/pallas_call | solution.py:334
